TPU v7x, 32 devices: a whole 2x2x4 slice. The times are simulated.
32 devices in a mesh: sp: 8 (over z, y), tp: 4 (over x, core).
Axes of the slice: x: 2, y: 2, z: 4, core: 2. Of those that a mesh axis runs over, the one named last changes fastest.
Arguments:
- memory_queries: bfloat16 [4096, 1024], P('sp', 'tp'), may hold values from -8 to 8
- memory_keys: bfloat16 [4096, 1024], P('sp', 'tp'), may hold values from -8 to 8
- memory_values: bfloat16 [4096, 1024], P('sp', 'tp'), may hold values from -6 to 6
- input_gate_logits: float32 [8, 4096], P('tp', 'sp'), may hold values from -64 to 160
- forget_gate_logits: float32 [8, 4096], P('tp', 'sp'), may hold values from -0.1 to 20
- extra_log_decay: float32 [8, 4096], P('tp', 'sp'), may hold values from -1.4 to 0
- residual: bfloat16 [4096, 2048], P(('sp', 'tp')), may hold values from -6 to 6
- cell_output_weight: bfloat16 [1024, 2048], P('tp', 'sp'), may hold values from -0.1875 to 0.1875
- expert_norm_gain: float32 [2048], replicated, may hold values from 0.1 to 1.9
- expert_gate_weight: bfloat16 [8, 2048, 3584], P('sp', None, 'tp'), may hold values from -0.125 to 0.125
- expert_up_weight: bfloat16 [8, 2048, 3584], P('sp', None, 'tp'), may hold values from -0.125 to 0.125
- expert_down_weight: bfloat16 [8, 3584, 2048], P('sp', 'tp'), may hold values from -0.09375 to 0.09375
- routed_expert_index: int32 [4096, 2], P('sp'), may hold values from 0 to 7, as said below
- routed_expert_weight: float32 [4096, 2], P(('sp', 'tp')), may hold values from 0.1 to 1
Outputs:
- layer_out: bfloat16 [4096, 2048], P(('sp', 'tp'))
Inputs may be any that keep to these rules, and one draw needn't show every extreme that they name: `routed_expert_index`: each row names 2 different experts. In each aligned block of 128 rows (the rows of one device after the cell) no expert is named more than 40 times, and one expert is named exactly 40 times in every block.
All inputs are finite; a program needn't handle non-finite values.
Results may differ from a plain program's by a relative error of at most 0.013.
Values may be sent and summed in bfloat16 or wider, within the bound.
A program may use at most 128 MiB of HBM per device.

v0:
```python
import jax
import jax.numpy as jnp
from jax import lax
from jax.sharding import PartitionSpec as P

highest = lax.Precision.HIGHEST
lowest = -1e30
epsilon = 1e-06


def carried_in(x, axis, combine, identity):
    length, place = (lax.axis_size(axis), lax.axis_index(axis))
    everything = jax.tree.map(lambda part: lax.all_gather(part, axis), x)
    start = jax.tree.map(
        lambda part, zero: jnp.broadcast_to(jnp.asarray(zero, part.dtype), part.shape), x, identity
    )

    def turn(k, before):
        reached = k < place
        new = combine(before, jax.tree.map(lambda part: part[k], everything))
        return jax.tree.map(lambda a, b: jnp.where(reached, a, b), new, before)

    return lax.fori_loop(0, length, turn, start)


def block_pass(memory, inputs):
    state_mat, state_norm, state_max = memory
    queries, keys_blk, values_blk, gate_in, forget_log_value = inputs
    length = gate_in.shape[-1]
    running = jnp.cumsum(forget_log_value, axis=-1)
    causal = jnp.arange(length)[:, None] >= jnp.arange(length)[None, :]
    exponent = running[:, :, None] - running[:, None, :] + gate_in[:, None, :]
    exponent = jnp.where(causal[None], exponent, -jnp.inf)
    carried = running + state_max[:, None]
    row_max = jnp.maximum(carried, jnp.max(exponent, axis=-1))
    decays = jnp.exp(exponent - row_max[:, :, None])
    carry_scale = jnp.exp(carried - row_max)
    dispatch_affinity = jnp.einsum("htk,hsk->hts", queries, keys_blk, precision=highest) * decays
    numerator = carry_scale[:, :, None] * jnp.einsum(
        "hvk,htk->htv", state_mat, queries, precision=highest
    )
    numerator = numerator + jnp.einsum(
        "hts,hsv->htv", dispatch_affinity, values_blk, precision=highest
    )
    denominator = carry_scale * jnp.einsum(
        "hk,htk->ht", state_norm, queries, precision=highest
    ) + jnp.sum(dispatch_affinity, axis=-1)
    final_log = running[:, -1]
    log_prev = final_log + state_max
    log_keep = final_log[:, None] - running + gate_in
    new_max = jnp.maximum(log_prev, jnp.max(log_keep, axis=-1))
    prev_scale = jnp.exp(log_prev - new_max)
    retain = jnp.exp(log_keep - new_max[:, None])
    new_mat = prev_scale[:, None, None] * state_mat + jnp.einsum(
        "hsv,hsk->hvk", retain[:, :, None] * values_blk, keys_blk, precision=highest
    )
    new_norm = prev_scale[:, None] * state_norm + jnp.einsum(
        "hs,hsk->hk", retain, keys_blk, precision=highest
    )
    return ((new_mat, new_norm, new_max), (numerator, denominator, row_max))


def join_states(earlier, later):
    early_log, early_mat, early_norm, early_max = earlier
    late_log, late_mat, late_norm, late_max = later
    joined_max = jnp.maximum(early_max + late_log, late_max)
    early_scale = jnp.exp(early_max + late_log - joined_max)
    late_scale = jnp.exp(late_max - joined_max)
    joined_mat = early_scale[:, None, None] * early_mat + late_scale[:, None, None] * late_mat
    joined_norm = early_scale[:, None] * early_norm + late_scale[:, None] * late_norm
    return (early_log + late_log, joined_mat, joined_norm, joined_max)


def matrix_memory_step(
    memory_queries,
    memory_keys,
    memory_values,
    input_gate_logits,
    forget_gate_logits,
    extra_log_decay,
):
    tokens_here, channels = memory_queries.shape
    heads_here = input_gate_logits.shape[0]
    head_dim = channels // heads_here

    def heads_first(tensor):
        return jnp.transpose(
            tensor.astype(jnp.float32).reshape(tokens_here, heads_here, head_dim), (1, 0, 2)
        )

    queries = heads_first(memory_queries) * head_dim ** (-0.5)
    forget_log_value = jax.nn.log_sigmoid(forget_gate_logits) + extra_log_decay
    block_size = min(tokens_here, 256)
    block_count = tokens_here // block_size

    def split_blocks(tensor):
        return jnp.moveaxis(
            tensor.reshape((heads_here, block_count, block_size) + tensor.shape[2:]), 1, 0
        )

    def join_blocks(tensor):
        return jnp.moveaxis(tensor, 0, 1).reshape((heads_here, tokens_here) + tensor.shape[3:])

    empty_state = (
        jnp.zeros((heads_here, head_dim, head_dim), jnp.float32),
        jnp.zeros((heads_here, head_dim), jnp.float32),
        jnp.full((heads_here,), lowest, jnp.float32),
    )
    members = (
        queries,
        heads_first(memory_keys),
        heads_first(memory_values),
        input_gate_logits,
        forget_log_value,
    )
    end_state, pieces = lax.scan(
        block_pass, empty_state, tuple((split_blocks(member) for member in members))
    )
    numerator, denominator, row_max = (join_blocks(member) for member in pieces)
    running = jnp.cumsum(forget_log_value, axis=-1)
    identity = (jnp.zeros((heads_here,), jnp.float32),) + empty_state
    incoming = carried_in((running[:, -1],) + tuple(end_state), "sp", join_states, identity)
    prior_mat, prior_norm, prior_max = incoming[1:]
    reached = running + prior_max[:, None]
    joined = jnp.maximum(row_max, reached)
    local_scale = jnp.exp(row_max - joined)
    carry_scale = jnp.exp(reached - joined)
    numerator = local_scale[:, :, None] * numerator + carry_scale[:, :, None] * jnp.einsum(
        "hvk,htk->htv", prior_mat, queries, precision=highest
    )
    denominator = local_scale * denominator + carry_scale * jnp.einsum(
        "hk,htk->ht", prior_norm, queries, precision=highest
    )
    guarded = jnp.maximum(jnp.abs(denominator), jnp.exp(-joined))
    return ((numerator / guarded[:, :, None]).astype(jnp.bfloat16), heads_here, head_dim)


def slot_index(ids, experts, capacity):
    flat_ids = ids.reshape(-1)
    matches = (flat_ids[:, None] == jnp.arange(experts, dtype=jnp.int32)[None, :]).astype(jnp.int32)
    before = jnp.cumsum(matches, axis=0) - matches
    return flat_ids * capacity + jnp.sum(before * matches, axis=1)


def local(
    memory_queries,
    memory_keys,
    memory_values,
    input_gate_logits,
    forget_gate_logits,
    extra_log_decay,
    residual,
    cell_output_weight,
    expert_norm_gain,
    expert_gate_weight,
    expert_up_weight,
    expert_down_weight,
    routed_expert_index,
    routed_expert_weight,
):
    hidden, heads_here, head_dim = matrix_memory_step(
        memory_queries,
        memory_keys,
        memory_values,
        input_gate_logits,
        forget_gate_logits,
        extra_log_decay,
    )
    weight_piece = lax.all_gather(cell_output_weight, "sp", axis=1, tiled=True)
    shaped = weight_piece.reshape(heads_here, head_dim, weight_piece.shape[1])
    partial_rows = jnp.einsum(
        "htd,hdc->tc", hidden, shaped, preferred_element_type=jnp.float32
    ).astype(jnp.bfloat16)
    projected = lax.psum_scatter(
        partial_rows.astype(jnp.float32).astype(jnp.bfloat16), "tp", scatter_dimension=0, tiled=True
    ).astype(jnp.float32)
    mixed_rows = (residual.astype(jnp.float32) + projected).astype(jnp.bfloat16)
    mixed_wide = mixed_rows.astype(jnp.float32)
    norm_scale = lax.rsqrt(jnp.mean(mixed_wide * mixed_wide, axis=-1, keepdims=True) + epsilon)
    normed = (mixed_wide * norm_scale * expert_norm_gain).astype(jnp.bfloat16)
    sp_size = lax.axis_size("sp")
    row_count, model_width = residual.shape
    top_count = routed_expert_index.shape[1]
    experts = sp_size * expert_gate_weight.shape[0]
    assigned = row_count * top_count
    capacity = max(2, assigned * 5 // (4 * experts))
    own_ids = lax.dynamic_slice_in_dim(
        routed_expert_index, lax.axis_index("tp") * row_count, row_count, 0
    )
    own_slots = slot_index(own_ids, experts, capacity)
    zero_row = jnp.zeros((1, model_width), jnp.bfloat16)
    padded = jnp.concatenate([normed, zero_row], axis=0)
    slot_table = jnp.full((experts * capacity,), row_count, jnp.int32)
    slot_table = slot_table.at[own_slots].set(jnp.arange(assigned, dtype=jnp.int32) // top_count)
    arrived = lax.all_gather(
        lax.all_to_all(
            padded[slot_table.reshape(experts, 1, capacity)],
            "sp",
            split_axis=0,
            concat_axis=0,
            tiled=True,
        ),
        "tp",
        axis=1,
        tiled=True,
    )
    sources, owners, slot_span, width_in = arrived.shape
    flat_rows = arrived.reshape(-1, width_in)
    gate_pre = jnp.dot(flat_rows, expert_gate_weight[0], preferred_element_type=jnp.float32)
    up_pre = jnp.dot(flat_rows, expert_up_weight[0], preferred_element_type=jnp.float32)
    hidden_act = (jax.nn.silu(gate_pre) * up_pre).astype(jnp.bfloat16)
    group_term = jnp.dot(hidden_act, expert_down_weight[0], preferred_element_type=jnp.float32)
    group_term = lax.optimization_barrier(group_term.astype(jnp.bfloat16)).astype(jnp.float32)
    summed = lax.psum_scatter(
        group_term.reshape(sources, owners, slot_span, width_in).astype(jnp.bfloat16),
        "tp",
        scatter_dimension=1,
        tiled=True,
    )
    returned = lax.all_to_all(summed, "sp", split_axis=0, concat_axis=0, tiled=True)
    picked = returned.reshape(experts * capacity, model_width)[own_slots]
    picked = picked.reshape(row_count, top_count, model_width).astype(jnp.float32)
    routed_sum = jnp.sum(picked * routed_expert_weight[:, :, None], axis=1)
    return (mixed_wide + routed_sum).astype(jnp.bfloat16)


def solution(mesh):
    return jax.shard_map(
        local,
        mesh=mesh,
        in_specs=(
            P("sp", "tp"),
            P("sp", "tp"),
            P("sp", "tp"),
            P("tp", "sp"),
            P("tp", "sp"),
            P("tp", "sp"),
            P(("sp", "tp"), None),
            P("tp", "sp"),
            P(),
            P("sp", None, "tp"),
            P("sp", None, "tp"),
            P("sp", "tp", None),
            P("sp", None),
            P(("sp", "tp"), None),
        ),
        out_specs=P(("sp", "tp"), None),
        check_vma=False,
    )
```

profile of v0, /device:TPU:0, one launch (start us, length us, event | category | flops | bytes accessed | tf_op | source)
XLA Modules:
  0.0 404.9 jit_solution(8255470432722626242)
XLA Ops:
  6.6 1.1 copy.56
  7.8 0.2 copy.57
  8.0 1.1 copy.54
  9.9 11.3 %while.39 = (s32[]{:T(128)}, f32[2,128,128]{2,1,0:T(8,128)S(1)}, f32[2,128]{1,0:T(2,128)S(1)}, f32[2]{0:T(128)S(1)}, f32[2,2,256,128]{3,2,0,1:T(8,128)S(1)}, /*i...) while((s32[]{:T(128)}, f32[2,128,128]{2,1,0:T(8,128)S(1)}, ...), condition=%wide.region_6.7_spmd.clone, body=%wide.region_0.6_spmd.clone.sunk | while | flops 607329536 | bytes 4625314 | solution.py:116
  9.9 0.6 reduce-window.38
  11.4 0.2 fusion.122
  11.7 0.6 fusion.123
  12.4 0.2 fusion.121
  12.7 0.3 fusion.124
  13.3 0.4 convolution_multiply_fusion.4
  13.6 1.0 fusion.125
  14.8 0.7 convolution_add_fusion.3
  15.6 0.6 reduce-window.38
  17.0 0.2 fusion.122
  17.3 0.6 fusion.123
  18.0 0.2 fusion.121
  18.4 0.3 fusion.124
  18.9 0.4 convolution_multiply_fusion.4
  19.3 1.0 fusion.125
  20.4 0.7 convolution_add_fusion.3
  21.2 0.6 copy-done
  21.9 0.7 all-gather.9.cloned.1.call-update
  22.7 0.6 reduce-window.22
  23.9 0.7 dynamic-slice
  25.3 0.2 dynamic-update-slice.1
  25.6 23.2 %all-reduce.4 = (f32[16]{0:T(128)S(1)}, f32[16]{0:T(128)S(1)}) all-reduce(f32[16]{0:T(128)S(1)} %bitcast_dynamic-update-slice_fusion.1, f32[16]{0:T(128)S(1)} %dynamic-update-slice.1), channel_id=2, replica_groups=mesh['sp'=8,'tp'=4] {'sp'}, use_global_device_ids=true, to_apply=%add.1 | all-reduce | flops 32 | bytes 256
  49.0 16.4 %all-gather.4 = f32[8,2,128]{2,1,0:T(2,128)S(1)} all-gather(f32[1,2,128]{2,1,0:T(2,128)S(1)} %bitcast.293), channel_id=5, replica_groups=mesh['sp'=8,'tp'=4] {'sp'}, dimensions={0}, use_global_device_ids=true | all-gather | bytes 9216 | tf_op jit(solution)/shard_map/all_gather | solution.py:13
  65.4 9.0 %while.40 = (s32[]{:T(128)}, f32[2,128,128]{2,1,0:T(8,128)S(1)}, f32[2,128]{1,0:T(2,128)S(1)}, f32[2]{0:T(128)S(1)}, s32[]{:T(128)}, /*index=5*/f32[8,2]{1,0:T(8...) while((s32[]{:T(128)}, f32[2,128,128]{2,1,0:T(8,128)S(1)}, ...), condition=%wide.region_10.11_spmd.clone, body=%wide.region_9.10_spmd.clone.sunk | while | flops 165138 | bytes 396541 | solution.py:23
  65.5 1.0 fusion.126
  66.6 1.0 fusion.126
  67.7 1.0 fusion.126
  68.8 1.0 fusion.126
  69.9 1.0 fusion.126
  71.1 1.0 fusion.126
  72.2 1.0 fusion.126
  73.3 1.0 fusion.126
  74.4 0.4 fusion.66
  74.9 0.2 bitcast_multiply_fusion.5
  75.1 1.2 fusion.47
  76.3 29.1 %all-gather.9.cloned.1.call-done = bf16[256,2048]{1,0:T(8,128)(2,1)} async-done(((bf16[256,256]{1,0:T(8,128)(2,1)}), bf16[256,2048]{1,0:T(8,128)(2,1)}) %all-gather.9.cloned.1.call-update) | async-done | bytes 1048592 | tf_op jit(solution)/shard_map/all_gather | solution.py:169
  105.3 3.3 bitcast_convert_fusion
  108.7 0.7 broadcast_multiply_fusion
  109.8 0.6 reduce-window.26
  110.4 0.2 slice_reduce_fusion.2
  111.0 1.4 scatter_custom_fusion
  112.6 26.4 %reduce-scatter.3.cloned.1.call-done = bf16[128,2048]{1,0:T(8,128)(2,1)} async-done(((bf16[512,2048]{1,0:T(8,128)(2,1)}), bf16[128,2048]{1,0:T(8,128)(2,1)}) %reduce-scatter.3.cloned.1.call-update) | async-done | bytes 524304 | tf_op jit(solution)/shard_map/reduce_scatter | solution.py:174
  139.0 1.3 fusion.48
  140.3 1.3 fusion.50
  141.6 2.4 gather_fusion
  144.0 36.6 %all_to_all.10 = bf16[8,1,40,2048]{3,2,1,0:T(8,128)(2,1)} all-to-all(bf16[8,1,40,2048]{3,2,1,0:T(8,128)(2,1)S(1)} %bitcast.275), channel_id=1, replica_groups=mesh['sp'=8,'tp'=4] {'sp'}, dimensions={0} | all-to-all | bytes 2621440 | tf_op jit(solution)/shard_map/all_to_all | solution.py:196
  180.7 0.2 all-reduce.7.cloned.1.call-start
  180.9 38.4 %all-gather.11.cloned.1.call-done = bf16[8,4,40,2048]{3,2,1,0:T(8,128)(2,1)} async-done(((bf16[8,1,40,2048]{3,2,1,0:T(8,128)(2,1)}), bf16[8,4,40,2048]{3,2,1,0:T(8,128)(2,1)}) %all-gather.11.cloned.1.call-update) | async-done | bytes 5242896 | tf_op jit(solution)/shard_map/all_gather | solution.py:195
  219.3 10.0 %fusion.43 = f32[1280,896]{1,0:T(8,128)} fusion(bf16[1280,2048]{1,0:T(8,128)(2,1)} %bitcast.302, bf16[1,2048,896]{2,1,0:T(8,128)(2,1)} %param.27), kind=kOutput, calls=%fused_computation.81 | convolution fusion | flops 4697620480 | bytes 13500416 | tf_op jit(solution)/shard_map/dot_general | solution.py:209
  229.3 17.6 %convolution_convert_fusion = bf16[1280,2048]{1,0:T(8,128)(2,1)} fusion(bf16[1,896,2048]{2,1,0:T(8,128)(2,1)} %param.29, f32[1280,896]{1,0:T(8,128)} %fusion.43, bf16[1280,2048]{1,0:T(8,128)(2,1)} %bitcast.303, bf16[1,2048,896]{2,1,0:T(8,128)(2,1)} %param.28), kind=kOutput, calls=%fused_computation.76 | convolution fusion | flops 9404743680 | bytes 22413312 | tf_op jit(solution)/shard_map/dot_general | solution.py:212
  246.9 0.6 copy-done.9
  247.5 0.6 dynamic-slice.2
  248.1 101.5 %all-reduce.7.cloned.1.call-done = bf16[8,4,40,2048]{3,2,1,0:T(8,128)(2,1)} async-done(((bf16[8,4,40,2048]{3,2,1,0:T(8,128)(2,1)}), bf16[8,4,40,2048]{3,2,1,0:T(8,128)(2,1)}) %all-reduce.7.cloned.1.call-update) | async-done | bytes 5242896
  349.6 3.2 constant_dynamic-slice_fusion.3
  352.8 5.5 %all-to-all-start.1 = ((bf16[8,1,40,2048]{3,2,1,0:T(8,128)(2,1)}), bf16[8,1,40,2048]{3,2,1,0:T(8,128)(2,1)S(1)}, u32[]{:S(2)}, u32[]{:S(2)}) async-start(bf16[8,1,40,2048]{3,2,1,0:T(8,128)(2,1)} %constant_dynamic-slice_fusion.3), calls=%async_computation.2 | async-start | bytes 2621440 | tf_op jit(solution)/shard_map/all_to_all | solution.py:220
  358.5 30.9 %all-to-all-done.1 = bf16[8,1,40,2048]{3,2,1,0:T(8,128)(2,1)S(1)} async-done(((bf16[8,1,40,2048]{3,2,1,0:T(8,128)(2,1)}), bf16[8,1,40,2048]{3,2,1,0:T(8,128)(2,1)S(1)}, u32[]{:S(2)}, u32[]{:S(2)}) %all-to-all-start.1) | async-done | bytes 1310752 | tf_op jit(solution)/shard_map/all_to_all | solution.py:220
  389.4 2.3 gather_fusion.1
  391.7 2.4 reshape.428
  394.2 3.2 multiply_reduce_fusion
  397.3 1.0 fusion.51
  (137 shorter events, 6.6 us)
Async XLA Ops:
  6.5 2.9 copy-start.3
  6.5 3.3 copy-start.7
  6.5 3.3 copy-start.6
  6.5 3.3 copy-start.4
  6.5 58.9 %all-gather.13.cloned.1.call-start = ((), (), s32[]{:S(2)}) async-start(), calls=%async_computation.6 | async-start | bytes 1179648 | tf_op jit(solution)/shard_map/all_gather | solution.py:13
  9.9 14.0 %copy-start.10 = (u32[32]{0:T(128)S(1)}, u32[32]{0:T(128)}, u32[]{:S(2)}) copy-start(u32[32]{0:T(128)} %constant.125) | copy-start | bytes 388
  21.2 0.7 copy-start
  21.8 83.5 %all-gather.9.cloned.1.call-start = ((), (), s32[]{:S(2)}) async-start(), calls=%async_computation.3 | async-start | bytes 1179648 | tf_op jit(solution)/shard_map/all_gather | solution.py:169
  22.6 116.4 %reduce-scatter.3.cloned.1.call-start = ((), (), s32[]{:S(2)}) async-start(), calls=%async_computation.4 | async-start | bytes 2621440 | tf_op jit(solution)/shard_map/reduce_scatter | solution.py:174
  75.1 63.9 %copy-start.1 = (bf16[128,2048]{1,0:T(8,128)(2,1)S(1)}, bf16[128,2048]{1,0:T(8,128)(2,1)}, u32[]{:S(2)}) copy-start(bf16[128,2048]{1,0:T(8,128)(2,1)} %param.24) | copy-start | bytes 1572868
  76.2 64.0 %copy-start.5 = (f32[2048]{0:T(1024)S(1)}, f32[2048]{0:T(1024)}, u32[]{:S(2)}) copy-start(f32[2048]{0:T(1024)} %param.26) | copy-start | bytes 24580
  108.6 110.7 %all-gather.11.cloned.1.call-start = ((), (), s32[]{:S(2)}) async-start(), calls=%async_computation.5 | async-start | bytes 6553600 | tf_op jit(solution)/shard_map/all_gather | solution.py:195
  180.7 168.9 %all-reduce.7.cloned.1.call-start = ((), (), s32[]{:S(2)}) async-start(), calls=%async_computation.7 | async-start | bytes 10485760
  246.9 0.7 copy-start.9
  246.9 111.4 %copy-start.8 = (f32[128,2]{0,1:T(2,128)S(1)}, f32[128,2]{0,1:T(2,128)}, u32[]{:S(2)}) copy-start(f32[128,2]{0,1:T(2,128)} %param.31) | copy-start | bytes 3076
  352.8 36.5 %all-to-all-start.1 = ((bf16[8,1,40,2048]{3,2,1,0:T(8,128)(2,1)}), bf16[8,1,40,2048]{3,2,1,0:T(8,128)(2,1)S(1)}, u32[]{:S(2)}, u32[]{:S(2)}) async-start(bf16[8,1,40,2048]{3,2,1,0:T(8,128)(2,1)} %constant_dynamic-slice_fusion.3), calls=%async_computation.2 | async-start | bytes 2621440 | tf_op jit(solution)/shard_map/all_to_all | solution.py:220
  391.7 5.6 %copy-start.2 = (bf16[128,2048]{1,0:T(8,128)(2,1)S(1)}, bf16[128,2048]{1,0:T(8,128)(2,1)}, u32[]{:S(2)}) copy-start(bf16[128,2048]{1,0:T(8,128)(2,1)} %reduce-scatter.3.cloned.1.call-done) | copy-start | bytes 1572868
Sparse Core Ops, SparseCore 0:
  22.0 43.1 all-gather.12
  67.2 38.0 all-gather.8
  108.8 30.1 reduce-scatter.2
  180.8 38.4 all-gather.10
  247.0 102.5 all-reduce.6
where the time goes:
time: 406 us; the launch traced here: 405 us
  waiting for transfers between devices  227 us (56%)
  blocking collectives  76.3 us (19%)
  matrix products  39.1 us (10%)
  other arithmetic  22 us (5%)
  local copies, waits for them, and re-layouts  20.1 us (5%)
  between operations  14.2 us (3%)
  starting transfers between devices  5.89 us (1%)
    unnamed x6, waiting for transfers between devices  102 us
    all_gather x1, waiting for transfers between devices, local(): lax.all_gather(lax.all_to_all(padded[slot_table.reshape(experts, 1, capac...  38.4 us
    all_to_all x1, blocking collectives, local(): lax.all_to_all(padded[slot_table.reshape(experts, 1, capacity)], 'sp', sp...  36.6 us
    all_to_all x1, waiting for transfers between devices, local(): lax.all_to_all(summed, 'sp', split_axis=0, concat_axis=0, tiled=True)  30.9 us
    all_gather x1, waiting for transfers between devices, local(): weight_piece = lax.all_gather(cell_output_weight, 'sp', axis=1, tiled=True)  29.1 us
    reduce_scatter x1, waiting for transfers between devices, local(): lax.psum_scatter(partial_rows.astype(jnp.float32).astype(jnp.bfloat16), '...  26.4 us
    unnamed x1, blocking collectives  23.2 us
    dot_general x1, matrix products, local(): jnp.dot(hidden_act, expert_down_weight[0], preferred_element_type=jnp.flo...  17.6 us
  transfers between devices with their start and end apart: 6, of which 5 were waited for; matrix products, arithmetic and copies ran while one was open for 4% of the time, Pallas kernels for 0%

commit v1 on v0

--- a/solution.py
+++ b/solution.py
@@ -166,7 +166,15 @@
         forget_gate_logits,
         extra_log_decay,
     )
-    weight_piece = lax.all_gather(cell_output_weight, "sp", axis=1, tiled=True)
+    n_dev = lax.axis_size("sp")
+    held, tiles = (cell_output_weight, [cell_output_weight])
+    for _ in range(n_dev - 1):
+        held = lax.ppermute(held, "sp", [(i, (i + 1) % n_dev) for i in range(n_dev)])
+        tiles.insert(0, held)
+    row_of_blocks = jnp.concatenate(tiles, axis=1)
+    weight_piece = jnp.roll(
+        row_of_blocks, (lax.axis_index("sp") + 1) * cell_output_weight.shape[1], axis=1
+    )
     shaped = weight_piece.reshape(heads_here, head_dim, weight_piece.shape[1])
     partial_rows = jnp.einsum(
         "htd,hdc->tc", hidden, shaped, preferred_element_type=jnp.float32

time: 406 us -> 416 us (1.025)
  local copies, waits for them, and re-layouts: 20.1 us -> 26.2 us
    ppermute x0 -> x7, waiting for transfers between devices: none -> 34.3 us  [local(): lax.ppermute(held, 'sp', [(i, (i + 1) % n_dev) for i in range(n_dev)])]
    all_gather x1 -> x0, waiting for transfers between devices: 29.1 us -> none  [local(): weight_piece = lax.all_gather(cell_output_weight, 'sp', axis=1, tiled=True)]
    unnamed x35 -> x54, local copies, waits for them, and re-layouts: 8.66 us -> 14.5 us
    unnamed x6 -> x5, waiting for transfers between devices: 102 us -> 102 us
  transfers between devices with their start and end apart: 6 -> 12, of which waited for: 5 -> 9; matrix products, arithmetic and copies ran while one was open for 4% -> 7% of each run, Pallas kernels for 0% -> 0%
where the time goes in v1:
time: 416 us; the launch traced here: 415 us
  waiting for transfers between devices  231 us (56%)
  blocking collectives  74.9 us (18%)
  matrix products  38 us (9%)
  local copies, waits for them, and re-layouts  26.2 us (6%)
  other arithmetic  22 us (5%)
  between operations  14.3 us (3%)
  starting transfers between devices  8.66 us (2%)
    unnamed x5, waiting for transfers between devices  102 us
    all_gather x1, waiting for transfers between devices, local(): lax.all_gather(lax.all_to_all(padded[slot_table.reshape(experts, 1, capac...  38.6 us
    all_to_all x1, blocking collectives, local(): lax.all_to_all(padded[slot_table.reshape(experts, 1, capacity)], 'sp', sp...  36.6 us
    ppermute x7, waiting for transfers between devices, local(): lax.ppermute(held, 'sp', [(i, (i + 1) % n_dev) for i in range(n_dev)])  34.3 us
    all_to_all x1, waiting for transfers between devices, local(): lax.all_to_all(summed, 'sp', split_axis=0, concat_axis=0, tiled=True)  30.9 us
    reduce_scatter x1, waiting for transfers between devices, local(): lax.psum_scatter(partial_rows.astype(jnp.float32).astype(jnp.bfloat16), '...  25.9 us
    unnamed x1, blocking collectives  21.9 us
    dot_general x1, matrix products, local(): jnp.dot(hidden_act, expert_down_weight[0], preferred_element_type=jnp.flo...  17.6 us
  transfers between devices with their start and end apart: 12, of which 9 were waited for; matrix products, arithmetic and copies ran while one was open for 7% of the time, Pallas kernels for 0%

profile of v1, /device:TPU:0, one launch (start us, length us, event | category | flops | bytes accessed | tf_op | source)
XLA Modules:
  0.0 415.5 jit_solution(683908669876277390)
XLA Ops:
  6.5 3.0 collective-permute-start
  9.5 1.1 copy.56
  11.1 5.2 %collective-permute-done = bf16[256,256]{1,0:T(8,128)(2,1)S(1)} collective-permute-done((bf16[256,256]{1,0:T(8,128)(2,1)}, bf16[256,256]{1,0:T(8,128)(2,1)S(1)}, u32[]{:S(2)}, u32[]{:S(2)}) %collective-permute-start) | collective-permute-done | bytes 131104 | tf_op jit(solution)/shard_map/ppermute | solution.py:172
  16.7 7.3 %collective-permute-done.1 = bf16[256,256]{1,0:T(8,128)(2,1)} collective-permute-done((bf16[256,256]{1,0:T(8,128)(2,1)S(1)}, bf16[256,256]{1,0:T(8,128)(2,1)}, u32[]{:S(2)}, u32[]{:S(2)}) %collective-permute-start.1) | collective-permute-done | bytes 131104 | tf_op jit(solution)/shard_map/ppermute | solution.py:172
  24.3 7.7 %collective-permute-done.2 = bf16[256,256]{1,0:T(8,128)(2,1)} collective-permute-done((bf16[256,256]{1,0:T(8,128)(2,1)}, bf16[256,256]{1,0:T(8,128)(2,1)}, u32[]{:S(2)}, u32[]{:S(2)}) %collective-permute-start.2) | collective-permute-done | bytes 131104 | tf_op jit(solution)/shard_map/ppermute | solution.py:172
  32.1 7.9 %collective-permute-done.3 = bf16[256,256]{1,0:T(8,128)(2,1)} collective-permute-done((bf16[256,256]{1,0:T(8,128)(2,1)}, bf16[256,256]{1,0:T(8,128)(2,1)}, u32[]{:S(2)}, u32[]{:S(2)}) %collective-permute-start.3) | collective-permute-done | bytes 131104 | tf_op jit(solution)/shard_map/ppermute | solution.py:172
  40.0 11.3 %while.39 = (s32[]{:T(128)}, f32[2,128,128]{2,1,0:T(8,128)S(1)}, f32[2,128]{1,0:T(2,128)S(1)}, f32[2]{0:T(128)S(1)}, f32[2,2,256,128]{3,2,0,1:T(8,128)S(1)}, /*i...) while((s32[]{:T(128)}, f32[2,128,128]{2,1,0:T(8,128)S(1)}, ...), condition=%wide.region_6.7_spmd.clone, body=%wide.region_0.6_spmd.clone.sunk | while | flops 607329536 | bytes 4625314 | solution.py:116
  40.1 0.6 reduce-window.38
  41.8 0.6 fusion.123
  42.9 0.3 fusion.124
  43.4 0.4 convolution_multiply_fusion.4
  43.8 1.1 fusion.125
  45.0 0.7 convolution_add_fusion.3
  45.7 0.6 reduce-window.38
  47.5 0.6 fusion.123
  49.1 0.4 convolution_multiply_fusion.4
  49.5 1.1 fusion.125
  50.6 0.7 convolution_add_fusion.3
  51.4 0.6 reduce-window.22
  52.6 0.7 dynamic-slice
  54.2 6.1 %collective-permute-done.5 = bf16[256,256]{1,0:T(8,128)(2,1)S(1)} collective-permute-done((bf16[256,256]{1,0:T(8,128)(2,1)}, bf16[256,256]{1,0:T(8,128)(2,1)S(1)}, u32[]{:S(2)}, u32[]{:S(2)}) %collective-permute-start.5) | collective-permute-done | bytes 131104 | tf_op jit(solution)/shard_map/ppermute | solution.py:172
  60.5 21.9 %all-reduce.4 = (f32[16]{0:T(128)S(1)}, f32[16]{0:T(128)S(1)}) all-reduce(f32[16]{0:T(128)S(1)} %bitcast_dynamic-update-slice_fusion.1, f32[16]{0:T(128)S(1)} %dynamic-update-slice.1), channel_id=2, replica_groups=mesh['sp'=8,'tp'=4] {'sp'}, use_global_device_ids=true, to_apply=%add.1 | all-reduce | flops 32 | bytes 256
  82.6 16.4 %all-gather.4 = f32[8,2,128]{2,1,0:T(2,128)S(1)} all-gather(f32[1,2,128]{2,1,0:T(2,128)S(1)} %bitcast.293), channel_id=5, replica_groups=mesh['sp'=8,'tp'=4] {'sp'}, dimensions={0}, use_global_device_ids=true | all-gather | bytes 9216 | tf_op jit(solution)/shard_map/all_gather | solution.py:13
  99.0 0.9 constant_dynamic-update-slice_fusion.13
  99.9 0.9 constant_dynamic-update-slice_fusion.12
  100.9 0.9 constant_dynamic-update-slice_fusion.11
  101.8 0.9 constant_dynamic-update-slice_fusion.10
  102.8 0.9 constant_dynamic-update-slice_fusion.5
  103.7 0.9 constant_dynamic-update-slice_fusion.4
  104.6 0.9 constant_dynamic-update-slice_fusion.3
  105.5 0.9 constant_dynamic-update-slice_fusion.2
  106.6 9.0 %while.40 = (s32[]{:T(128)}, f32[2,128,128]{2,1,0:T(8,128)S(1)}, f32[2,128]{1,0:T(2,128)S(1)}, f32[2]{0:T(128)S(1)}, s32[]{:T(128)}, /*index=5*/f32[8,2]{1,0:T(8...) while((s32[]{:T(128)}, f32[2,128,128]{2,1,0:T(8,128)S(1)}, ...), condition=%wide.region_10.11_spmd.clone, body=%wide.region_9.10_spmd.clone.sunk | while | flops 165138 | bytes 396541 | solution.py:23
  106.7 1.0 fusion.126
  107.8 1.0 fusion.126
  108.9 1.0 fusion.126
  110.1 1.0 fusion.126
  111.2 1.0 fusion.126
  112.3 1.0 fusion.126
  113.4 1.0 fusion.126
  114.5 1.0 fusion.126
  115.6 0.4 fusion.66
  116.3 1.2 fusion.47
  117.5 2.1 bitcast_convert_fusion
  119.6 0.7 broadcast_multiply_fusion
  120.8 0.6 reduce-window.26
  122.0 1.6 scatter_custom_fusion
  123.7 25.9 %reduce-scatter.3.cloned.1.call-done = bf16[128,2048]{1,0:T(8,128)(2,1)} async-done(((bf16[512,2048]{1,0:T(8,128)(2,1)}), bf16[128,2048]{1,0:T(8,128)(2,1)}) %reduce-scatter.3.cloned.1.call-update) | async-done | bytes 524304 | tf_op jit(solution)/shard_map/reduce_scatter | solution.py:182
  149.6 1.3 fusion.48
  150.9 1.2 fusion.50
  152.2 2.4 gather_fusion
  154.7 36.6 %all_to_all.10 = bf16[8,1,40,2048]{3,2,1,0:T(8,128)(2,1)} all-to-all(bf16[8,1,40,2048]{3,2,1,0:T(8,128)(2,1)S(1)} %bitcast.275), channel_id=1, replica_groups=mesh['sp'=8,'tp'=4] {'sp'}, dimensions={0} | all-to-all | bytes 2621440 | tf_op jit(solution)/shard_map/all_to_all | solution.py:204
  191.4 38.6 %all-gather.8.cloned.1.call-done = bf16[8,4,40,2048]{3,2,1,0:T(8,128)(2,1)} async-done(((bf16[8,1,40,2048]{3,2,1,0:T(8,128)(2,1)}), bf16[8,4,40,2048]{3,2,1,0:T(8,128)(2,1)}) %all-gather.8.cloned.1.call-update) | async-done | bytes 5242896 | tf_op jit(solution)/shard_map/all_gather | solution.py:203
  230.0 10.0 %fusion.43 = f32[1280,896]{1,0:T(8,128)} fusion(bf16[1280,2048]{1,0:T(8,128)(2,1)} %bitcast.302, bf16[1,2048,896]{2,1,0:T(8,128)(2,1)} %param.27), kind=kOutput, calls=%fused_computation.81 | convolution fusion | flops 4697620480 | bytes 13500416 | tf_op jit(solution)/shard_map/dot_general | solution.py:217
  240.0 17.6 %convolution_convert_fusion = bf16[1280,2048]{1,0:T(8,128)(2,1)} fusion(bf16[1,896,2048]{2,1,0:T(8,128)(2,1)} %param.29, f32[1280,896]{1,0:T(8,128)} %fusion.43, bf16[1280,2048]{1,0:T(8,128)(2,1)} %bitcast.303, bf16[1,2048,896]{2,1,0:T(8,128)(2,1)} %param.28), kind=kOutput, calls=%fused_computation.76 | convolution fusion | flops 9404743680 | bytes 22413312 | tf_op jit(solution)/shard_map/dot_general | solution.py:220
  257.5 0.6 copy-done.11
  258.2 0.6 dynamic-slice.2
  258.8 101.5 %all-reduce.7.cloned.1.call-done = bf16[8,4,40,2048]{3,2,1,0:T(8,128)(2,1)} async-done(((bf16[8,4,40,2048]{3,2,1,0:T(8,128)(2,1)}), bf16[8,4,40,2048]{3,2,1,0:T(8,128)(2,1)}) %all-reduce.7.cloned.1.call-update) | async-done | bytes 5242896
  360.2 3.2 constant_dynamic-slice_fusion.3
  363.5 5.5 %all-to-all-start.1 = ((bf16[8,1,40,2048]{3,2,1,0:T(8,128)(2,1)}), bf16[8,1,40,2048]{3,2,1,0:T(8,128)(2,1)S(1)}, u32[]{:S(2)}, u32[]{:S(2)}) async-start(bf16[8,1,40,2048]{3,2,1,0:T(8,128)(2,1)} %constant_dynamic-slice_fusion.3), calls=%async_computation.2 | async-start | bytes 2621440 | tf_op jit(solution)/shard_map/all_to_all | solution.py:228
  369.1 30.9 %all-to-all-done.1 = bf16[8,1,40,2048]{3,2,1,0:T(8,128)(2,1)S(1)} async-done(((bf16[8,1,40,2048]{3,2,1,0:T(8,128)(2,1)}), bf16[8,1,40,2048]{3,2,1,0:T(8,128)(2,1)S(1)}, u32[]{:S(2)}, u32[]{:S(2)}) %all-to-all-start.1) | async-done | bytes 1310752 | tf_op jit(solution)/shard_map/all_to_all | solution.py:228
  400.0 2.3 gather_fusion.1
  402.4 2.4 reshape.428
  404.7 3.2 multiply_reduce_fusion
  407.9 1.0 fusion.51
  (169 shorter events, 9.1 us)
Async XLA Ops:
  6.5 4.4 %copy-start.4 = (bf16[512,256]{1,0:T(8,128)(2,1)S(1)}, bf16[512,256]{1,0:T(8,128)(2,1)}, u32[]{:S(2)}) copy-start(bf16[512,256]{1,0:T(8,128)(2,1)} %param.19) | copy-start | bytes 786436
  6.5 100.1 %all-gather.10.cloned.1.call-start = ((), (), s32[]{:S(2)}) async-start(), calls=%async_computation.5 | async-start | bytes 1179648 | tf_op jit(solution)/shard_map/all_gather | solution.py:13
  6.5 9.7 %collective-permute-start = (bf16[256,256]{1,0:T(8,128)(2,1)}, bf16[256,256]{1,0:T(8,128)(2,1)S(1)}, u32[]{:S(2)}, u32[]{:S(2)}) collective-permute-start(bf16[256,256]{1,0:T(8,128)(2,1)} %param.25), channel_id=1, source_target_pairs={{0,4},{4,8},{8,12},{12,16},{16,20},{20,24},{24,28},{28,0},{1,5},{5... | collective-permute-start | bytes 393224 | tf_op jit(solution)/shard_map/ppermute | solution.py:172
  10.6 5.9 %copy-start.5 = (bf16[512,256]{1,0:T(8,128)(2,1)S(1)}, bf16[512,256]{1,0:T(8,128)(2,1)}, u32[]{:S(2)}) copy-start(bf16[512,256]{1,0:T(8,128)(2,1)} %param.20) | copy-start | bytes 786436
  16.3 7.8 %collective-permute-start.1 = (bf16[256,256]{1,0:T(8,128)(2,1)S(1)}, bf16[256,256]{1,0:T(8,128)(2,1)}, u32[]{:S(2)}, u32[]{:S(2)}) collective-permute-start(bf16[256,256]{1,0:T(8,128)(2,1)S(1)} %collective-permute-done), channel_id=1, source_target_pairs={{0,4},{4,8},{8,12},{12,16},{16,20},{20,24},{24,28},{28,0},{1,5},{5... | collective-permute-start | bytes 393224 | tf_op jit(solution)/shard_map/ppermute | solution.py:172
  16.3 15.8 %copy-start.8 = (f32[2,512]{1,0:T(2,128)S(1)}, f32[2,512]{1,0:T(2,128)}, u32[]{:S(2)}) copy-start(f32[2,512]{1,0:T(2,128)} %param.23) | copy-start | bytes 12292
  16.3 15.8 %copy-start.9 = (f32[2,512]{1,0:T(2,128)S(1)}, f32[2,512]{1,0:T(2,128)}, u32[]{:S(2)}) copy-start(f32[2,512]{1,0:T(2,128)} %param.22) | copy-start | bytes 12292
  16.3 23.7 %copy-start.6 = (f32[2,512]{1,0:T(2,128)S(1)}, f32[2,512]{1,0:T(2,128)}, u32[]{:S(2)}) copy-start(f32[2,512]{1,0:T(2,128)} %param.21) | copy-start | bytes 12292
  24.0 8.0 %collective-permute-start.2 = (bf16[256,256]{1,0:T(8,128)(2,1)}, bf16[256,256]{1,0:T(8,128)(2,1)}, u32[]{:S(2)}, u32[]{:S(2)}) collective-permute-start(bf16[256,256]{1,0:T(8,128)(2,1)} %collective-permute-done.1), channel_id=1, source_target_pairs={{0,4},{4,8},{8,12},{12,16},{16,20},{20,24},{24,28},{28,0},{1,5},{5... | collective-permute-start | bytes 393224 | tf_op jit(solution)/shard_map/ppermute | solution.py:172
  32.0 8.0 %collective-permute-start.3 = (bf16[256,256]{1,0:T(8,128)(2,1)}, bf16[256,256]{1,0:T(8,128)(2,1)}, u32[]{:S(2)}, u32[]{:S(2)}) collective-permute-start(bf16[256,256]{1,0:T(8,128)(2,1)} %collective-permute-done.2), channel_id=1, source_target_pairs={{0,4},{4,8},{8,12},{12,16},{16,20},{20,24},{24,28},{28,0},{1,5},{5... | collective-permute-start | bytes 393224 | tf_op jit(solution)/shard_map/ppermute | solution.py:172
  40.0 12.4 %collective-permute-start.4 = (bf16[256,256]{1,0:T(8,128)(2,1)}, bf16[256,256]{1,0:T(8,128)(2,1)}, u32[]{:S(2)}, u32[]{:S(2)}) collective-permute-start(bf16[256,256]{1,0:T(8,128)(2,1)} %collective-permute-done.3), channel_id=1, source_target_pairs={{0,4},{4,8},{8,12},{12,16},{16,20},{20,24},{24,28},{28,0},{1,5},{5... | collective-permute-start | bytes 393224 | tf_op jit(solution)/shard_map/ppermute | solution.py:172
  40.0 12.6 %copy-start.12 = (u32[32]{0:T(128)S(1)}, u32[32]{0:T(128)}, u32[]{:S(2)}) copy-start(u32[32]{0:T(128)} %constant.149) | copy-start | bytes 388
  51.4 9.1 %copy-start = (f32[2,128,128]{2,1,0:T(8,128)}, f32[2,128,128]{2,1,0:T(8,128)S(1)}, u32[]{:S(2)}) copy-start(f32[2,128,128]{2,1,0:T(8,128)S(1)} %get-tuple-element.230) | copy-start | bytes 393220
  51.4 51.3 %copy-start.3 = (bf16[256,256]{1,0:T(8,128)(2,1)S(1)}, bf16[256,256]{1,0:T(8,128)(2,1)}, u32[]{:S(2)}) copy-start(bf16[256,256]{1,0:T(8,128)(2,1)} %param.25) | copy-start | bytes 393220
  52.4 8.0 %collective-permute-start.5 = (bf16[256,256]{1,0:T(8,128)(2,1)}, bf16[256,256]{1,0:T(8,128)(2,1)S(1)}, u32[]{:S(2)}, u32[]{:S(2)}) collective-permute-start(bf16[256,256]{1,0:T(8,128)(2,1)} %collective-permute-done.4), channel_id=1, source_target_pairs={{0,4},{4,8},{8,12},{12,16},{16,20},{20,24},{24,28},{28,0},{1,5},{5... | collective-permute-start | bytes 393224 | tf_op jit(solution)/shard_map/ppermute | solution.py:172
  60.3 38.6 %collective-permute-start.6 = (bf16[256,256]{1,0:T(8,128)(2,1)S(1)}, bf16[256,256]{1,0:T(8,128)(2,1)S(1)}, u32[]{:S(2)}, u32[]{:S(2)}) collective-permute-start(bf16[256,256]{1,0:T(8,128)(2,1)S(1)} %collective-permute-done.5), channel_id=1, source_target_pairs={{0,4},{4,8},{8,12},{12,16},{16,20},{20,24},{24,28},{28,0},{1,5},{5... | collective-permute-start | bytes 393224 | tf_op jit(solution)/shard_map/ppermute | solution.py:172
  60.5 89.2 %reduce-scatter.3.cloned.1.call-start = ((), (), s32[]{:S(2)}) async-start(), calls=%async_computation.3 | async-start | bytes 2621440 | tf_op jit(solution)/shard_map/reduce_scatter | solution.py:182
  119.6 30.1 %copy-start.1 = (bf16[128,2048]{1,0:T(8,128)(2,1)S(1)}, bf16[128,2048]{1,0:T(8,128)(2,1)}, u32[]{:S(2)}) copy-start(bf16[128,2048]{1,0:T(8,128)(2,1)} %param.24) | copy-start | bytes 1572868
  119.6 31.4 %copy-start.7 = (f32[2048]{0:T(1024)S(1)}, f32[2048]{0:T(1024)}, u32[]{:S(2)}) copy-start(f32[2048]{0:T(1024)} %param.26) | copy-start | bytes 24580
  119.6 110.4 %all-gather.8.cloned.1.call-start = ((), (), s32[]{:S(2)}) async-start(), calls=%async_computation.4 | async-start | bytes 6553600 | tf_op jit(solution)/shard_map/all_gather | solution.py:203
  191.3 168.9 %all-reduce.7.cloned.1.call-start = ((), (), s32[]{:S(2)}) async-start(), calls=%async_computation.6 | async-start | bytes 10485760
  257.5 0.7 copy-start.11
  360.2 8.7 %copy-start.10 = (f32[128,2]{0,1:T(2,128)S(1)}, f32[128,2]{0,1:T(2,128)}, u32[]{:S(2)}) copy-start(f32[128,2]{0,1:T(2,128)} %param.31) | copy-start | bytes 3076
  363.5 36.5 %all-to-all-start.1 = ((bf16[8,1,40,2048]{3,2,1,0:T(8,128)(2,1)}), bf16[8,1,40,2048]{3,2,1,0:T(8,128)(2,1)S(1)}, u32[]{:S(2)}, u32[]{:S(2)}) async-start(bf16[8,1,40,2048]{3,2,1,0:T(8,128)(2,1)} %constant_dynamic-slice_fusion.3), calls=%async_computation.2 | async-start | bytes 2621440 | tf_op jit(solution)/shard_map/all_to_all | solution.py:228
  404.7 3.2 copy-start.2
Sparse Core Ops, SparseCore 0:
  60.6 41.8 all-gather.9
  119.7 29.8 reduce-scatter.2
  191.5 38.4 all-gather.7
  257.7 102.5 all-reduce.6
